TPU v7x, 32 devices: a whole 2x2x4 slice. The times are simulated.
32 devices in a mesh: sp: 8 (over z, x), tp: 4 (over y, core).
Axes of the slice: x: 2, y: 2, z: 4, core: 2. Of those that a mesh axis runs over, the one named last changes fastest.
Arguments:
- hidden_in: bfloat16 [2, 12288, 2048], P(None, ('sp', 'tp')), may hold values from -6 to 6
- w_value: bfloat16 [2048, 2048], P(None, 'tp'), may hold values from -0.125 to 0.125
- w_key: bfloat16 [2048, 2048], P(None, 'tp'), may hold values from -0.125 to 0.125
- w_step: bfloat16 [2048, 32], replicated, may hold values from -0.125 to 0.125
- conv_value: bfloat16 [4, 2048], P(None, 'tp'), may hold values from -3 to 3
- conv_key: bfloat16 [4, 2048], P(None, 'tp'), may hold values from -3 to 3
- step_bias: float32 [32], P('tp'), may hold values from -3 to -1
- decay_rate: float32 [32], P('tp'), may hold values from 8.138021e-06 to 0.25
- decay_jump: float32 [2, 12288, 32], P(None, 'sp', 'tp'), may hold values from -0.75 to 0
- new_value: bfloat16 [2, 2048], P(None, 'tp'), may hold values from -60 to 60
- new_key: bfloat16 [2, 2048], P(None, 'tp'), may hold values from -6 to 6
- new_query: bfloat16 [2, 2048], P(None, 'tp'), may hold values from -6 to 6
- new_gate: bfloat16 [2, 2048], P(None, 'tp'), may hold values from -6 to 6
- new_step: float32 [2, 32], P(None, 'tp'), may hold values from -6 to 6
- read_gain: bfloat16 [2048], P('tp'), may hold values from 0.099609375 to 1.8984375
Outputs:
- prompt_state: bfloat16 [2, 32, 64, 128], P(None, 'tp', 'sp')
- read_out: bfloat16 [2, 32, 64], P(None, 'tp', 'sp')
All inputs are finite; a program needn't handle non-finite values.
Results may differ from a plain program's by a relative error of at most 0.006.
Values may be sent and summed in bfloat16 or wider, within the bound.
A program may use at most 64 MiB of HBM per device.

v0:
```python
import jax
import jax.numpy as jnp
from jax import lax
from jax.experimental import pallas as pl
from jax.experimental.pallas import tpu as pltpu
from jax.sharding import PartitionSpec as P

HEAD_DIM = 64
STATE = 128


EPSILON = 1e-05


def shifted(value, axis, steps):
    count = lax.axis_size(axis)
    leading, last = (max(0, -steps), min(count, count - steps))
    return lax.ppermute(value, axis, [(source, source + steps) for source in range(leading, last)])


def causal_mix(padded_rows, conv_taps):
    tap_count = conv_taps.shape[0]
    length = padded_rows.shape[-2] - tap_count + 1
    running = jnp.zeros(padded_rows.shape[:-2] + (length, padded_rows.shape[-1]), jnp.float32)
    for tap_index in range(tap_count):
        running = running + padded_rows[..., tap_index : tap_index + length, :].astype(
            jnp.float32
        ) * conv_taps[tap_index].astype(jnp.float32)
    return running


def block_states(mixed_rows, weight, value_cols, groups_dev):
    seq_count, row_count, heads_dev = weight.shape
    per_group = heads_dev // groups_dev
    values = (
        mixed_rows[:, :, :value_cols].reshape(seq_count, row_count, groups_dev, per_group, HEAD_DIM)
        * weight.reshape(seq_count, row_count, groups_dev, per_group)[..., None]
    )
    keys = mixed_rows[:, :, value_cols:].reshape(seq_count, row_count, groups_dev, STATE)
    states = jnp.einsum("slgep,slgn->sgepn", values, keys, precision=lax.Precision.HIGHEST)
    return states.reshape(seq_count, heads_dev, HEAD_DIM, STATE)


def general(
    hidden_in,
    w_value,
    w_key,
    w_step,
    conv_value,
    conv_key,
    step_bias,
    decay_rate,
    decay_jump,
    new_value,
    new_key,
    new_query,
    new_gate,
    new_step,
    read_gain,
):
    sp_count = lax.axis_size("sp")
    sp_index = lax.axis_index("sp")
    tp_index = lax.axis_index("tp")
    heads_dev = step_bias.shape[0]
    value_cols = w_value.shape[1]
    key_cols = w_key.shape[1]
    groups_dev = key_cols // STATE
    per_group = heads_dev // groups_dev
    kernel_taps = conv_value.shape[0]
    seq_count = hidden_in.shape[0]
    share = HEAD_DIM // sp_count
    own_step = lax.dynamic_slice_in_dim(w_step, tp_index * heads_dev, heads_dev, 1)
    w_joined = jnp.concatenate([w_value, w_key, own_step], axis=1)
    projected = jnp.einsum(
        "tfy,yz->tfz",
        lax.all_gather(hidden_in, "tp", axis=1, tiled=True),
        w_joined,
        preferred_element_type=jnp.float32,
    ).astype(jnp.bfloat16)
    seg_rows = projected.shape[1]
    proj_pair = projected[:, :, : value_cols + key_cols]
    proj_step = projected[:, :, value_cols + key_cols :]
    step_size = jax.nn.softplus(proj_step.astype(jnp.float32) + step_bias)
    log_decay = decay_jump - decay_rate * step_size
    conv_taps = jnp.concatenate([conv_value, conv_key], axis=1)
    edge_rows = shifted(proj_pair[:, seg_rows - (kernel_taps - 1) :, :], "sp", 1)
    mixed_rows = jax.nn.silu(causal_mix(jnp.concatenate([edge_rows, proj_pair], axis=1), conv_taps))
    seg_total = jnp.sum(log_decay, axis=1)
    decay_after = seg_total[:, None, :] - jnp.cumsum(log_decay, axis=1)
    seg_states = block_states(mixed_rows, step_size * jnp.exp(decay_after), value_cols, groups_dev)
    tiled_totals = jnp.broadcast_to(
        seg_total[:, None, :, None], (seq_count, 1, heads_dev, sp_count)
    )
    got_states, got_totals = (
        lax.all_to_all(seg_states[:, None], "sp", split_axis=3, concat_axis=1, tiled=True),
        lax.all_to_all(tiled_totals, "sp", split_axis=3, concat_axis=1, tiled=True),
    )
    got_totals = got_totals[..., 0]
    tail_decay = jnp.sum(got_totals, axis=1, keepdims=True) - jnp.cumsum(got_totals, axis=1)
    final_state = jnp.einsum(
        "sjh,sjhpn->shpn", jnp.exp(tail_decay), got_states, precision=lax.Precision.HIGHEST
    )
    cache_state = final_state.astype(jnp.bfloat16)
    new_size = jax.nn.softplus(new_step + step_bias)
    keep_share = jnp.exp(-decay_rate * new_size)
    query = new_query.astype(jnp.float32).reshape(seq_count, groups_dev, STATE)
    own_key = new_key.astype(jnp.float32).reshape(seq_count, groups_dev, STATE)
    key_match = jnp.sum(own_key * query, axis=-1)
    size_grid = new_size.reshape(seq_count, groups_dev, per_group)
    keep_grid = keep_share.reshape(seq_count, groups_dev, per_group)
    value_grid = new_value.astype(jnp.float32).reshape(seq_count, groups_dev, per_group, HEAD_DIM)
    gate_grid = jax.nn.silu(new_gate.astype(jnp.float32)).reshape(
        seq_count, groups_dev, per_group, HEAD_DIM
    )
    gain_grid = read_gain.astype(jnp.float32).reshape(groups_dev, per_group, HEAD_DIM)
    own_value = lax.dynamic_slice_in_dim(value_grid, sp_index * share, share, 3)
    own_gate = lax.dynamic_slice_in_dim(gate_grid, sp_index * share, share, 3)
    own_gain = lax.dynamic_slice_in_dim(gain_grid, sp_index * share, share, 2)
    state_read = jnp.einsum(
        "sgepn,sgn->sgep",
        final_state.reshape(seq_count, groups_dev, per_group, share, STATE),
        query,
        precision=lax.Precision.HIGHEST,
    )
    raw_read = (
        keep_grid[..., None] * state_read
        + size_grid[..., None] * own_value * key_match[:, :, None, None]
    )
    gated = raw_read * own_gate
    squares = lax.psum(jnp.sum(gated * gated, axis=(2, 3)), "sp")
    scale = lax.rsqrt(squares / (per_group * HEAD_DIM) + EPSILON)
    read_out = (gated * scale[:, :, None, None] * own_gain).astype(jnp.bfloat16)
    return (cache_state, read_out.reshape(seq_count, heads_dev, share))


MESH = pl.DeviceIdType.MESH
PIECES = 4
ROW_TILE = 64
EDGE = 16


def softplus(x):
    return jnp.maximum(x, 0.0) + jnp.log1p(jnp.exp(-jnp.abs(x)))


def flip(value, bit):
    return value + bit - 2 * bit * ((value // bit) % 2)


def mixer_kernel(
    hid, wv, wk, wstep, taps, bias_rate, jump, query, coef,
    state_out, read_out,
    rows, w_all, tall, jall, ball, qall, step_t, wx, proj, val, key, totals, stage, full, got, reads, read_got,
    hid_local, hid_send, hid_recv, w_local, edge_send, edge_recv, small_send, small_recv,
    y_send, x_send, z_send, w_recv, tot_send, tot_recv, st_send, st_recv, rd_send, rd_recv,
):
    sp, tp = lax.axis_index("sp"), lax.axis_index("tp")
    sp_count = lax.axis_size("sp")
    y, core = tp // 2, tp % 2
    far = 1 - y
    chips = 2 * sp_count
    seqs, part, width = hid.shape
    local = 2 * part
    depth = width // PIECES
    groups = w_all.shape[1]
    heads = jump.shape[1]
    share = 64 // sp_count
    per_share = stage.shape[3] // seqs
    quarter = sp % 4

    def xor_sp(bits):
        out, bit = sp, 1
        while bit < sp_count:
            if bits & bit:
                out = flip(out, bit)
            bit *= 2
        return out

    x_peer, z_peer, y_peer = (flip(sp, 1), tp), (flip(sp, 2), tp), (sp, flip(tp, 2))
    core_peer = (sp, flip(tp, 1))

    def chip_peer(r):
        return (xor_sp(r % sp_count), flip(tp, 2) if r >= sp_count else tp)

    def send(src, dst, send_sem, recv_sem, peer):
        return pltpu.make_async_remote_copy(
            src_ref=src, dst_ref=dst, send_sem=send_sem, recv_sem=recv_sem, device_id=peer, device_id_type=MESH
        )

    order = sp * 2 + y
    after = lax.rem(order + 1, chips)
    next_chip = (after // 2, (after % 2) * 2 + core)

    barrier = pltpu.get_barrier_semaphore()
    for r in range(1, chips):
        pl.semaphore_signal(barrier, inc=1, device_id=chip_peer(r), device_id_type=MESH)
    pl.semaphore_signal(barrier, inc=1, device_id=core_peer, device_id_type=MESH)

    mine = pl.ds(pl.multiple_of(EDGE + core * part, 16), part)
    load_hid = [pltpu.make_async_copy(hid.at[s], rows.at[s, mine, :], hid_local.at[s]) for s in range(seqs)]
    load_w = [
        pltpu.make_async_copy(
            w.at[:, pl.ds(a * 128, 128)], w_all.at[y, a, half], w_local.at[a, half]
        )
        for a in range(groups)
        for half, w in enumerate((wv, wk))
    ]
    for c in load_hid + load_w:
        c.start()
    jall[y] = jump[:, :, pl.ds(pl.multiple_of(y * local, 128), local)]
    ball[y] = bias_rate[...]
    tall[y] = taps[...]
    qall[y] = query[...]
    reads[...] = jnp.zeros(reads.shape, jnp.float32)
    pl.semaphore_wait(barrier, chips)

    send_hid = [
        send(hid.at[s], rows.at[s, mine, :], hid_send.at[s], hid_recv.at[s], core_peer) for s in range(seqs)
    ]
    theirs = pl.ds(pl.multiple_of(far * local, 128), local)
    send_small = [
        send(jump.at[:, :, theirs], jall.at[y], small_send.at[0], small_recv.at[0], y_peer),
        send(bias_rate, ball.at[y], small_send.at[1], small_recv.at[1], y_peer),
        send(taps, tall.at[y], small_send.at[2], small_recv.at[2], y_peer),
        send(query, qall.at[y], small_send.at[3], small_recv.at[3], y_peer),
    ]
    count = 2 * PIECES
    diag = groups - 1 - quarter
    first, second = (3 * count) // 8, (6 * count) // 8
    y_list = [(quarter, chunk, 0) for chunk in range(count)] + [(diag, chunk, 3) for chunk in range(second, count)]
    send_y = [
        send(
            (wv, wk)[chunk % 2].at[pl.ds((chunk // 2) * depth, depth), pl.ds(pl.multiple_of(a * 128, 128), 128)],
            w_all.at[y, a, chunk % 2, pl.ds((chunk // 2) * depth, depth), :],
            y_send.at[n], w_recv.at[rel, chunk], y_peer,
        )
        for n, (a, chunk, rel) in enumerate(y_list)
    ]
    for c in send_hid + send_small + send_y:
        c.start()

    def w_copy(a, chunk, send_sem, rel, peer):
        block = w_all.at[
            far, a, chunk % 2, pl.ds(pl.multiple_of((chunk // 2) * depth, depth), depth), :
        ]
        return send(block, block, send_sem, w_recv.at[rel, chunk], peer)

    def wait_chunk(rel, a, chunk):
        w_copy(a, chunk, y_send.at[0], rel, y_peer).wait_recv()

    def relay(chunk):
        wait_chunk(0, quarter, chunk)
        w_copy(quarter, chunk, x_send.at[chunk], 1, x_peer).start()
        w_copy(quarter, chunk, z_send.at[chunk], 2, z_peer).start()

    qx, qz = flip(quarter, 1), flip(quarter, 2)

    def relay_diag(n):
        wait_chunk(1, qx, n)
        w_copy(qx, n, z_send.at[count + n], 3, z_peer).start()
        wait_chunk(2, qz, first + n)
        w_copy(qz, first + n, x_send.at[count + n], 3, x_peer).start()

    for c in load_hid:
        c.wait()
    for c in send_hid:
        c.wait_recv()
    edge = send(
        rows.at[:, pl.ds(local, EDGE), :], rows.at[:, pl.ds(0, EDGE), :], edge_send, edge_recv, next_chip
    )
    edge.start()
    relay(0)
    for s in range(seqs):
        step_t[s] = (
            lax.dot_general(
                wstep[...], rows[s, EDGE:, :], (((1,), (1,)), ((), ())), preferred_element_type=jnp.float32
            )
            .astype(jnp.bfloat16)
            .astype(jnp.float32)
        )
    for c in send_small:
        c.wait_recv()
    decays, sizes = [], []
    for yb in range(2):
        for s in range(seqs):
            raw = step_t[s, pl.ds(pl.multiple_of((2 * yb + core) * heads, 8), heads), :]
            one = softplus(raw + ball[yb, :, 0:1])
            sizes.append(one)
            decays.append(jall[yb, s] - ball[yb, :, 1:2] * one)
    size = jnp.concatenate(sizes, axis=0)
    decay = jnp.concatenate(decays, axis=0)
    column = lax.broadcasted_iota(jnp.int32, (heads, 128), 1)
    packed = jnp.zeros((heads, 128), jnp.float32)
    for n, one in enumerate(decays):
        packed = jnp.where(column == n, jnp.sum(one, axis=1, keepdims=True), packed)
    totals[0] = packed
    relay(1)
    send_tot = [
        send(totals.at[0], totals.at[r], tot_send.at[r], tot_recv.at[r], chip_peer(r)) for r in range(1, chips)
    ]
    for c in send_tot:
        c.start()
    spot = lax.broadcasted_iota(jnp.int32, decay.shape, 1)
    suffix = jnp.where(spot < local - 1, pltpu.roll(decay, local - 1, 1), 0.0)
    shift = 1
    while shift < local:
        suffix = suffix + jnp.where(spot < local - shift, pltpu.roll(suffix, local - shift, 1), 0.0)
        shift *= 2
    edge.wait_recv()

    @pl.when(order == 0)
    def _():
        rows[:, 0:EDGE, :] = jnp.zeros((seqs, EDGE, width), rows.dtype)

    relay(2)
    later = jnp.zeros((heads, 128), jnp.float32)
    for r in range(1, chips):
        send_tot[r - 1].wait_recv()
        source = xor_sp(r % sp_count) * 2 + (far if r >= sp_count else y)
        later = later + totals[r] * jnp.where(source > order, 1.0, 0.0)
    later = jnp.concatenate([later[:, n : n + 1] for n in range(len(decays))], axis=0)
    weight_t = (size * jnp.exp(suffix + later)).T
    lane = lax.broadcasted_iota(jnp.int32, (local, 128), 1)
    for yb in range(2):
        for s in range(seqs):
            for a in range(groups):
                at = (yb * seqs + s) * heads + 2 * a
                wx[yb, s, a] = jnp.where(lane < 64, weight_t[:, at : at + 1], weight_t[:, at + 1 : at + 2])
    for c in load_w:
        c.wait()

    def step(slot, block, a, s):
        proj[...] = (
            jnp.dot(rows[s], jnp.concatenate([w_all[block, a, 0], w_all[block, a, 1]], axis=1), preferred_element_type=jnp.float32)
            .astype(jnp.bfloat16)
            .astype(jnp.float32)
        )
        tap = tall[block, a]

        def mix(i, carry):
            base = pl.multiple_of(i * ROW_TILE, ROW_TILE)
            span = proj[pl.ds(base + 8, ROW_TILE + 8), :]
            acc = span[5 : 5 + ROW_TILE] * tap[0:1]
            for k in range(1, 4):
                acc = acc + span[5 + k : 5 + k + ROW_TILE] * tap[k : k + 1]
            acc = acc / (1.0 + jnp.exp(-acc))
            here = pl.ds(base, ROW_TILE)
            val[here, :] = (acc[:, :128] * wx[block, s, a, here, :]).astype(jnp.bfloat16)
            key[here, :] = acc[:, 128:].astype(jnp.bfloat16)
            return carry

        lax.fori_loop(0, local // ROW_TILE, mix, 0)
        state = lax.dot_general(
            val[...], key[...], (((0,), (0,)), ((), ())), preferred_element_type=jnp.float32
        )
        per = state.shape[0] // 64
        parts = jnp.swapaxes(state.reshape(per, sp_count, share, 128), 0, 1).reshape(sp_count, per_share, 128)
        here = pl.ds(pl.multiple_of(s * per_share, per_share), per_share)
        stage[slot, a, :, here, :] = parts.astype(jnp.bfloat16)
        line = a * seqs + s
        read = lax.dot_general(
            qall[block, line], state, (((1,), (1,)), ((), ())),
            precision=lax.Precision.HIGHEST, preferred_element_type=jnp.float32,
        )
        reads[slot] = jnp.where(lax.broadcasted_iota(jnp.int32, read.shape, 0) == line, read, reads[slot])
        if slot == 0:
            full[a, :, here, :] = parts

    def send_states(slot, a, peers):
        for r in peers:
            send(
                stage.at[slot, a, xor_sp(r % sp_count)], got.at[r - 1, a], st_send, st_recv, chip_peer(r)
            ).start()

    ready = 3

    def own_block(j, carry):
        a, s = j // seqs, j % seqs

        @pl.when(j < count - ready)
        def _():
            relay(j + ready)

        @pl.when(j >= count - ready)
        def _():
            relay_diag(j - (count - ready))

        step(0, y, a, s)

        @pl.when(s == seqs - 1)
        def _():
            send_states(0, a, range(1, sp_count))

        return carry

    lax.fori_loop(0, groups * seqs, own_block, 0)

    def send_reads(slot, r):
        return send(reads.at[slot], read_got.at[r], rd_send.at[r], rd_recv.at[r], chip_peer(r))

    waits = {
        1: list(range(first, count)),
        2: list(range(first)) + list(range(second, count)),
        3: list(range(count)),
    }

    def far_block(j, carry):
        k, s = j // seqs, j % seqs
        a = (quarter % 2 + k % 2) % 2 + 2 * ((quarter // 2 + k // 2) % 2)
        for rel, chunks in waits.items():

            @pl.when(j == rel * seqs)
            def _():
                for chunk in chunks:
                    wait_chunk(rel, a, chunk)

        @pl.when(j == 1)
        def _():
            for r in range(1, sp_count):
                send_reads(0, r).start()

        step(1, far, a, s)

        @pl.when(s == seqs - 1)
        def _():
            send_states(1, a, range(sp_count, chips))

        return carry

    lax.fori_loop(0, groups * seqs, far_block, 0)

    send_rd = [send_reads(r // sp_count, r) for r in range(1, chips)]
    for c in send_rd[sp_count - 1 :]:
        c.start()
    everything = send(got, got, st_send, st_recv, y_peer)
    everything.wait_recv()
    for a in range(groups):
        final = full[a, sp]
        for r in range(chips - 1):
            final = final + got[r, a].astype(jnp.float32)
        state_out[a] = final
    read = reads[0]
    for r in range(1, chips):
        send_rd[r - 1].wait_recv()
        read = read + read_got[r]
    gated = coef[0] * read + coef[1]
    mean = jnp.mean(gated * gated, axis=1, keepdims=True)
    read_out[...] = gated * lax.rsqrt(mean + EPSILON) * coef[2]
    for c in send_hid + send_small + send_y + [edge] + send_tot + send_rd + [everything]:
        c.wait_send()
    for n in range(count):
        w_copy(quarter, n, x_send.at[n], 1, x_peer).wait_send()
        w_copy(quarter, n, z_send.at[n], 2, z_peer).wait_send()
    for n in range(first):
        w_copy(qx, n, z_send.at[count + n], 3, z_peer).wait_send()
        w_copy(qz, n, x_send.at[count + n], 3, x_peer).wait_send()


def per_device(
    hidden_in, w_value, w_key, w_step, conv_value, conv_key, step_bias, decay_rate, decay_jump,
    new_value, new_key, new_query, new_gate, new_step, read_gain,
):
    sp_count, tp_count = lax.axis_size("sp"), lax.axis_size("tp")
    heads = step_bias.shape[0]
    groups = w_key.shape[1] // STATE
    seqs, part, width = hidden_in.shape
    per = heads // groups
    share = HEAD_DIM // sp_count
    if not (tp_count == 4 and groups == 4 and share == 8 and per == 2 and seqs == 2 and part % 64 == 0):
        return general(
            hidden_in, w_value, w_key, w_step, conv_value, conv_key, step_bias, decay_rate, decay_jump,
            new_value, new_key, new_query, new_gate, new_step, read_gain,
        )
    f32 = jnp.float32
    sp_index = lax.axis_index("sp")
    local = 2 * part
    tap_count = conv_value.shape[0]
    taps = jnp.concatenate(
        [conv_value.reshape(tap_count, groups, 128), conv_key.reshape(tap_count, groups, 128)], axis=2
    )
    taps = jnp.pad(jnp.swapaxes(taps, 0, 1).astype(f32), ((0, 0), (0, 8 - tap_count), (0, 0)))
    bias_rate = jnp.pad(jnp.stack([step_bias, decay_rate], axis=1), ((0, 0), (0, 126)))

    def lines_of(x):
        return jnp.swapaxes(x.astype(f32).reshape(seqs, groups, -1), 0, 1)

    def per_channel(x):
        return jnp.repeat(lines_of(x), HEAD_DIM, axis=2)

    query = lines_of(new_query)
    key_match = jnp.sum(lines_of(new_key) * query, axis=-1, keepdims=True)
    new_size = jax.nn.softplus(new_step + step_bias)
    gate = jax.nn.silu(lines_of(new_gate))
    coef = jnp.stack(
        [
            per_channel(jnp.exp(-decay_rate * new_size)) * gate,
            per_channel(new_size) * lines_of(new_value) * key_match * gate,
            jnp.broadcast_to(read_gain.astype(f32).reshape(groups, 1, per * HEAD_DIM), gate.shape),
        ]
    ).reshape(3, groups * seqs, per * HEAD_DIM)
    query = jnp.broadcast_to(query.reshape(groups * seqs, 1, STATE), (groups * seqs, 8, STATE))
    chips = 2 * sp_count
    bf16 = jnp.bfloat16
    block = seqs * per * share
    vmem, anyspace = pl.BlockSpec(memory_space=pltpu.VMEM), pl.BlockSpec(memory_space=pl.ANY)
    dma = pltpu.SemaphoreType.DMA
    count = 2 * PIECES
    state, read = pl.pallas_call(
        mixer_kernel,
        out_shape=(
            jax.ShapeDtypeStruct((groups, block, 128), f32),
            jax.ShapeDtypeStruct((groups * seqs, 128), f32),
        ),
        in_specs=[anyspace] * 3 + [vmem] * 6,
        out_specs=(vmem, vmem),
        scratch_shapes=[
            pltpu.VMEM((seqs, EDGE + local, width), bf16),
            pltpu.VMEM((2, groups, 2, width, 128), bf16),
            pltpu.VMEM((2, groups, 8, 256), f32),
            pltpu.VMEM((2, seqs, heads, local), f32),
            pltpu.VMEM((2, heads, 128), f32),
            pltpu.VMEM((2, groups * seqs, 8, STATE), f32),
            pltpu.VMEM((seqs, 4 * heads, local), f32),
            pltpu.VMEM((2, seqs, groups, local, 128), f32),
            pltpu.VMEM((EDGE + local, 256), f32),
            pltpu.VMEM((local, 128), bf16),
            pltpu.VMEM((local, 128), bf16),
            pltpu.VMEM((chips, heads, 128), f32),
            pltpu.VMEM((2, groups, sp_count, block, 128), bf16),
            pltpu.VMEM((groups, sp_count, block, 128), f32),
            pltpu.VMEM((chips - 1, groups, block, 128), bf16),
            pltpu.VMEM((2, groups * seqs, 128), f32),
            pltpu.VMEM((chips, groups * seqs, 128), f32),
            dma((seqs,)), dma((seqs,)), dma((seqs,)), dma((groups, 2)), dma, dma, dma((4,)), dma((4,)),
            dma((2 * count,)), dma((2 * count,)), dma((2 * count,)), dma((4, count)),
            dma((chips,)), dma((chips,)), dma, dma, dma((chips,)), dma((chips,)),
        ],
        compiler_params=pltpu.CompilerParams(
            collective_id=0, has_side_effects=True, vmem_limit_bytes=60 * 1024 * 1024
        ),
    )(
        hidden_in, w_value, w_key, jnp.swapaxes(w_step, 0, 1), taps, bias_rate,
        jnp.swapaxes(decay_jump, 1, 2), query, coef,
    )

    state = jnp.swapaxes(state.reshape(groups, seqs, per, share, STATE), 0, 1)
    read = lax.dynamic_slice_in_dim(read.reshape(groups, seqs, per, HEAD_DIM), sp_index * share, share, 3)
    read = jnp.swapaxes(read, 0, 1)
    return (
        state.reshape(seqs, heads, share, STATE).astype(bf16),
        read.reshape(seqs, heads, share).astype(bf16),
    )


def solution(mesh):
    return jax.shard_map(
        per_device,
        mesh=mesh,
        in_specs=(
            P(None, ("sp", "tp"), None),
            P(None, "tp"),
            P(None, "tp"),
            P(),
            P(None, "tp"),
            P(None, "tp"),
            P("tp"),
            P("tp"),
            P(None, "sp", "tp"),
            P(None, "tp"),
            P(None, "tp"),
            P(None, "tp"),
            P(None, "tp"),
            P(None, "tp"),
            P("tp"),
        ),
        out_specs=(P(None, "tp", "sp", None), P(None, "tp", "sp")),
        check_vma=False,
    )
```

profile of v0, /device:TPU:0, one launch (start us, length us, event | category | flops | bytes accessed | tf_op | source)
XLA Modules:
  0.0 108.9 jit_solution(18161987715986569356)
XLA Ops:
  0.6 0.7 maximum_bitcast_fusion
  1.3 0.6 pad_convert_fusion.taps
  2.0 0.7 pad_maximum_fusion.1
  2.6 0.1 copy.43
  2.7 0.6 pad.12.bias_rate
  3.3 0.7 bitcast_convert_fusion
  4.0 0.6 broadcast_in_dim.17.query
  4.6 0.7 bitcast_convert_fusion.1
  5.3 0.7 neg.11
  6.0 0.7 multiply_exponential_fusion
  6.7 0.1 reshape.74
  6.7 0.1 broadcast_in_dim.19
  6.8 0.1 reshape.75
  6.9 0.8 fusion.2
  7.7 0.1 reshape.71
  7.8 0.1 broadcast_in_dim.18
  7.9 0.1 reshape.72
  8.0 0.7 fusion.13
  8.7 0.6 pad_maximum_fusion.coef
  9.3 96.7 %shard_map.158 = (f32[4,32,128]{2,1,0:T(8,128)}, f32[8,128]{1,0:T(8,128)}) custom-call(bf16[2,384,2048]{2,1,0:T(8,128)(2,1)} %hid.1, bf16[2048,512]{1,0:T(8,128)(2,1)} %wv.1, bf16[2048,512]{1,0:T(8,128)(2,1)} %wk.1, bf16[32,2048]{1,0:T(8,128)(2,1)} %bitcast.85, f32[4,8,256]{2,1,0:T(8,128)} %pad_convert_fusion.taps, f32[8,128]{1,0:T(8,128)} %pad.12.bias_rate, ...), custom_call_target="tpu_custom_call" | custom-call | tf_op jit(solution)/shard_map/pallas_call | solution.py:508
  106.0 0.8 convert_element_type.35
  106.8 0.6 copy.52
  107.4 0.8 reshape.78
  108.2 0.1 constant_dynamic-slice_fusion
  108.3 0.6 copy.57
  (3 shorter events, 0.0 us)
where the time goes:
time: 109 us
  Pallas kernels  96.7 us (89%)
  other arithmetic  7.71 us (7%)
  local copies, waits for them, and re-layouts  3.85 us (4%)
    pallas_call x1, Pallas kernels, per_device(): pl.pallas_call(mixer_kernel, out_shape=(jax.ShapeDtypeStruct((groups, blo...  96.7 us

commit v1 on v0

--- a/solution.py
+++ b/solution.py
@@ -189,12 +189,19 @@
 
     order = sp * 2 + y
     after = lax.rem(order + 1, chips)
-    next_chip = (after // 2, (after % 2) * 2 + core)
 
     barrier = pltpu.get_barrier_semaphore()
     for r in range(1, chips):
         pl.semaphore_signal(barrier, inc=1, device_id=chip_peer(r), device_id_type=MESH)
     pl.semaphore_signal(barrier, inc=1, device_id=core_peer, device_id_type=MESH)
+    before = lax.rem(order + chips - 1, chips)
+
+    @pl.when(core == 0)
+    def _():
+        pl.semaphore_signal(
+            barrier, inc=1, device_id=(before // 2, (before % 2) * 2 + 1), device_id_type=MESH
+        )
+
 
     mine = pl.ds(pl.multiple_of(EDGE + core * part, 16), part)
     load_hid = [pltpu.make_async_copy(hid.at[s], rows.at[s, mine, :], hid_local.at[s]) for s in range(seqs)]
@@ -212,7 +219,7 @@
     tall[y] = taps[...]
     qall[y] = query[...]
     reads[...] = jnp.zeros(reads.shape, jnp.float32)
-    pl.semaphore_wait(barrier, chips)
+    pl.semaphore_wait(barrier, chips + core)
 
     send_hid = [
         send(hid.at[s], rows.at[s, mine, :], hid_send.at[s], hid_recv.at[s], core_peer) for s in range(seqs)
@@ -236,7 +243,20 @@
         )
         for n, (a, chunk, rel) in enumerate(y_list)
     ]
-    for c in send_hid + send_small + send_y:
+    edge = [
+        send(
+            hid.at[:, pl.ds(part - EDGE, EDGE), :], rows.at[:, pl.ds(0, EDGE), :], edge_send.at[c], edge_recv,
+            (after // 2, (after % 2) * 2 + c),
+        )
+        for c in range(2)
+    ]
+
+    @pl.when(core == 1)
+    def _():
+        for c in edge:
+            c.start()
+
+    for c in send_hid + send_y[:1] + send_small + send_y[1:]:
         c.start()
 
     def w_copy(a, chunk, send_sem, rel, peer):
@@ -265,10 +285,6 @@
         c.wait()
     for c in send_hid:
         c.wait_recv()
-    edge = send(
-        rows.at[:, pl.ds(local, EDGE), :], rows.at[:, pl.ds(0, EDGE), :], edge_send, edge_recv, next_chip
-    )
-    edge.start()
     relay(0)
     for s in range(seqs):
         step_t[s] = (
@@ -306,7 +322,7 @@
     while shift < local:
         suffix = suffix + jnp.where(spot < local - shift, pltpu.roll(suffix, local - shift, 1), 0.0)
         shift *= 2
-    edge.wait_recv()
+    edge[0].wait_recv()
 
     @pl.when(order == 0)
     def _():
@@ -446,7 +462,12 @@
     gated = coef[0] * read + coef[1]
     mean = jnp.mean(gated * gated, axis=1, keepdims=True)
     read_out[...] = gated * lax.rsqrt(mean + EPSILON) * coef[2]
-    for c in send_hid + send_small + send_y + [edge] + send_tot + send_rd + [everything]:
+    @pl.when(core == 1)
+    def _():
+        for c in edge:
+            c.wait_send()
+
+    for c in send_hid + send_small + send_y + send_tot + send_rd + [everything]:
         c.wait_send()
     for n in range(count):
         w_copy(quarter, n, x_send.at[n], 1, x_peer).wait_send()
@@ -531,7 +552,7 @@
             pltpu.VMEM((chips - 1, groups, block, 128), bf16),
             pltpu.VMEM((2, groups * seqs, 128), f32),
             pltpu.VMEM((chips, groups * seqs, 128), f32),
-            dma((seqs,)), dma((seqs,)), dma((seqs,)), dma((groups, 2)), dma, dma, dma((4,)), dma((4,)),
+            dma((seqs,)), dma((seqs,)), dma((seqs,)), dma((groups, 2)), dma((2,)), dma, dma((4,)), dma((4,)),
             dma((2 * count,)), dma((2 * count,)), dma((2 * count,)), dma((4, count)),
             dma((chips,)), dma((chips,)), dma, dma, dma((chips,)), dma((chips,)),
         ],

time: 109 us -> 109 us (level)
  no operation moved by 1% of the time
where the time goes in v1:
time: 109 us; the launch traced here: 108 us
  Pallas kernels  96.1 us (88%)
  other arithmetic  7.71 us (7%)
  local copies, waits for them, and re-layouts  3.85 us (4%)
    pallas_call x1, Pallas kernels, per_device(): pl.pallas_call(mixer_kernel, out_shape=(jax.ShapeDtypeStruct((groups, blo...  96.1 us

profile of v1, /device:TPU:0, one launch (start us, length us, event | category | flops | bytes accessed | tf_op | source)
XLA Modules:
  0.0 108.3 jit_solution(15190436796763417255)
XLA Ops:
  0.6 0.7 maximum_bitcast_fusion
  1.3 0.6 pad_convert_fusion.taps
  2.0 0.7 pad_maximum_fusion.1
  2.6 0.1 copy.43
  2.7 0.6 pad.12.bias_rate
  3.3 0.7 bitcast_convert_fusion
  4.0 0.6 broadcast_in_dim.17.query
  4.6 0.7 bitcast_convert_fusion.1
  5.3 0.7 neg.11
  6.0 0.7 multiply_exponential_fusion
  6.7 0.1 reshape.74
  6.7 0.1 broadcast_in_dim.19
  6.8 0.1 reshape.75
  6.9 0.8 fusion.2
  7.7 0.1 reshape.71
  7.8 0.1 broadcast_in_dim.18
  7.9 0.1 reshape.72
  8.0 0.7 fusion.13
  8.7 0.6 pad_maximum_fusion.coef
  9.3 96.1 %shard_map.158 = (f32[4,32,128]{2,1,0:T(8,128)}, f32[8,128]{1,0:T(8,128)}) custom-call(bf16[2,384,2048]{2,1,0:T(8,128)(2,1)} %hid.1, bf16[2048,512]{1,0:T(8,128)(2,1)} %wv.1, bf16[2048,512]{1,0:T(8,128)(2,1)} %wk.1, bf16[32,2048]{1,0:T(8,128)(2,1)} %bitcast.85, f32[4,8,256]{2,1,0:T(8,128)} %pad_convert_fusion.taps, f32[8,128]{1,0:T(8,128)} %pad.12.bias_rate, ...), custom_call_target="tpu_custom_call" | custom-call | tf_op jit(solution)/shard_map/pallas_call | solution.py:529
  105.4 0.8 convert_element_type.35
  106.3 0.6 copy.52
  106.9 0.8 reshape.78
  107.7 0.1 constant_dynamic-slice_fusion
  107.7 0.6 copy.57
  (3 shorter events, 0.0 us)

commit v2 on v1

v2 whole, which is shorter than its diff:
```python
import jax
import jax.numpy as jnp
from jax import lax
from jax.experimental import pallas as pl
from jax.experimental.pallas import tpu as pltpu
from jax.sharding import PartitionSpec as P

HEAD_DIM = 64
STATE = 128


EPSILON = 1e-05


def shifted(value, axis, steps):
    count = lax.axis_size(axis)
    leading, last = (max(0, -steps), min(count, count - steps))
    return lax.ppermute(value, axis, [(source, source + steps) for source in range(leading, last)])


def causal_mix(padded_rows, conv_taps):
    tap_count = conv_taps.shape[0]
    length = padded_rows.shape[-2] - tap_count + 1
    running = jnp.zeros(padded_rows.shape[:-2] + (length, padded_rows.shape[-1]), jnp.float32)
    for tap_index in range(tap_count):
        running = running + padded_rows[..., tap_index : tap_index + length, :].astype(
            jnp.float32
        ) * conv_taps[tap_index].astype(jnp.float32)
    return running


def block_states(mixed_rows, weight, value_cols, groups_dev):
    seq_count, row_count, heads_dev = weight.shape
    per_group = heads_dev // groups_dev
    values = (
        mixed_rows[:, :, :value_cols].reshape(seq_count, row_count, groups_dev, per_group, HEAD_DIM)
        * weight.reshape(seq_count, row_count, groups_dev, per_group)[..., None]
    )
    keys = mixed_rows[:, :, value_cols:].reshape(seq_count, row_count, groups_dev, STATE)
    states = jnp.einsum("slgep,slgn->sgepn", values, keys, precision=lax.Precision.HIGHEST)
    return states.reshape(seq_count, heads_dev, HEAD_DIM, STATE)


def general(
    hidden_in,
    w_value,
    w_key,
    w_step,
    conv_value,
    conv_key,
    step_bias,
    decay_rate,
    decay_jump,
    new_value,
    new_key,
    new_query,
    new_gate,
    new_step,
    read_gain,
):
    sp_count = lax.axis_size("sp")
    sp_index = lax.axis_index("sp")
    tp_index = lax.axis_index("tp")
    heads_dev = step_bias.shape[0]
    value_cols = w_value.shape[1]
    key_cols = w_key.shape[1]
    groups_dev = key_cols // STATE
    per_group = heads_dev // groups_dev
    kernel_taps = conv_value.shape[0]
    seq_count = hidden_in.shape[0]
    share = HEAD_DIM // sp_count
    own_step = lax.dynamic_slice_in_dim(w_step, tp_index * heads_dev, heads_dev, 1)
    w_joined = jnp.concatenate([w_value, w_key, own_step], axis=1)
    projected = jnp.einsum(
        "tfy,yz->tfz",
        lax.all_gather(hidden_in, "tp", axis=1, tiled=True),
        w_joined,
        preferred_element_type=jnp.float32,
    ).astype(jnp.bfloat16)
    seg_rows = projected.shape[1]
    proj_pair = projected[:, :, : value_cols + key_cols]
    proj_step = projected[:, :, value_cols + key_cols :]
    step_size = jax.nn.softplus(proj_step.astype(jnp.float32) + step_bias)
    log_decay = decay_jump - decay_rate * step_size
    conv_taps = jnp.concatenate([conv_value, conv_key], axis=1)
    edge_rows = shifted(proj_pair[:, seg_rows - (kernel_taps - 1) :, :], "sp", 1)
    mixed_rows = jax.nn.silu(causal_mix(jnp.concatenate([edge_rows, proj_pair], axis=1), conv_taps))
    seg_total = jnp.sum(log_decay, axis=1)
    decay_after = seg_total[:, None, :] - jnp.cumsum(log_decay, axis=1)
    seg_states = block_states(mixed_rows, step_size * jnp.exp(decay_after), value_cols, groups_dev)
    tiled_totals = jnp.broadcast_to(
        seg_total[:, None, :, None], (seq_count, 1, heads_dev, sp_count)
    )
    got_states, got_totals = (
        lax.all_to_all(seg_states[:, None], "sp", split_axis=3, concat_axis=1, tiled=True),
        lax.all_to_all(tiled_totals, "sp", split_axis=3, concat_axis=1, tiled=True),
    )
    got_totals = got_totals[..., 0]
    tail_decay = jnp.sum(got_totals, axis=1, keepdims=True) - jnp.cumsum(got_totals, axis=1)
    final_state = jnp.einsum(
        "sjh,sjhpn->shpn", jnp.exp(tail_decay), got_states, precision=lax.Precision.HIGHEST
    )
    cache_state = final_state.astype(jnp.bfloat16)
    new_size = jax.nn.softplus(new_step + step_bias)
    keep_share = jnp.exp(-decay_rate * new_size)
    query = new_query.astype(jnp.float32).reshape(seq_count, groups_dev, STATE)
    own_key = new_key.astype(jnp.float32).reshape(seq_count, groups_dev, STATE)
    key_match = jnp.sum(own_key * query, axis=-1)
    size_grid = new_size.reshape(seq_count, groups_dev, per_group)
    keep_grid = keep_share.reshape(seq_count, groups_dev, per_group)
    value_grid = new_value.astype(jnp.float32).reshape(seq_count, groups_dev, per_group, HEAD_DIM)
    gate_grid = jax.nn.silu(new_gate.astype(jnp.float32)).reshape(
        seq_count, groups_dev, per_group, HEAD_DIM
    )
    gain_grid = read_gain.astype(jnp.float32).reshape(groups_dev, per_group, HEAD_DIM)
    own_value = lax.dynamic_slice_in_dim(value_grid, sp_index * share, share, 3)
    own_gate = lax.dynamic_slice_in_dim(gate_grid, sp_index * share, share, 3)
    own_gain = lax.dynamic_slice_in_dim(gain_grid, sp_index * share, share, 2)
    state_read = jnp.einsum(
        "sgepn,sgn->sgep",
        final_state.reshape(seq_count, groups_dev, per_group, share, STATE),
        query,
        precision=lax.Precision.HIGHEST,
    )
    raw_read = (
        keep_grid[..., None] * state_read
        + size_grid[..., None] * own_value * key_match[:, :, None, None]
    )
    gated = raw_read * own_gate
    squares = lax.psum(jnp.sum(gated * gated, axis=(2, 3)), "sp")
    scale = lax.rsqrt(squares / (per_group * HEAD_DIM) + EPSILON)
    read_out = (gated * scale[:, :, None, None] * own_gain).astype(jnp.bfloat16)
    return (cache_state, read_out.reshape(seq_count, heads_dev, share))


MESH = pl.DeviceIdType.MESH
PIECES = 4
EDGE = 16
TIP = 8


def softplus(x):
    return jnp.maximum(x, 0.0) + jnp.log1p(jnp.exp(-jnp.abs(x)))


def flip(value, bit):
    return value + bit - 2 * bit * ((value // bit) % 2)


def mixer_kernel(
    hid, wv, wk, wstep, cv, ck, jump, newv, newk, newq, newg, bias, rate, newstep,
    state_out, read_out,
    rows, w_all, wst, ctap, tall, jall, ball, nraw, qraw, qall, coef, step_t, wrow, proj, sfull, fac, totals,
    stage, full, got, reads, read_got,
    hid_local, hid_send, hid_recv, w_local, small_local, edge_send, edge_recv, small_send, small_recv,
    y_send, x_send, z_send, w_recv, tot_send, tot_recv, st_send, st_recv, rd_send, rd_recv,
):
    sp, tp = lax.axis_index("sp"), lax.axis_index("tp")
    sp_count = lax.axis_size("sp")
    y, core = tp // 2, tp % 2
    far = 1 - y
    chips = 2 * sp_count
    seqs, part, width = hid.shape
    local = 2 * part
    depth = width // PIECES
    groups = w_all.shape[1]
    heads = jump.shape[1]
    lines = groups * seqs
    share = 64 // sp_count
    per_share = stage.shape[3] // seqs
    quarter = sp % 4
    f32, bf16 = jnp.float32, jnp.bfloat16

    def xor_sp(bits):
        out, bit = sp, 1
        while bit < sp_count:
            if bits & bit:
                out = flip(out, bit)
            bit *= 2
        return out

    x_peer, z_peer, y_peer = (flip(sp, 1), tp), (flip(sp, 2), tp), (sp, flip(tp, 2))
    core_peer = (sp, flip(tp, 1))

    def chip_peer(r):
        return (xor_sp(r % sp_count), flip(tp, 2) if r >= sp_count else tp)

    def send(src, dst, send_sem, recv_sem, peer):
        return pltpu.make_async_remote_copy(
            src_ref=src, dst_ref=dst, send_sem=send_sem, recv_sem=recv_sem, device_id=peer, device_id_type=MESH
        )

    order = sp * 2 + y
    after = lax.rem(order + 1, chips)
    before = lax.rem(order + chips - 1, chips)

    barrier = pltpu.get_barrier_semaphore()
    for r in range(1, chips):
        pl.semaphore_signal(barrier, inc=1, device_id=chip_peer(r), device_id_type=MESH)
    pl.semaphore_signal(barrier, inc=1, device_id=core_peer, device_id_type=MESH)

    @pl.when(core == 0)
    def _():
        pl.semaphore_signal(barrier, inc=1, device_id=(before // 2, (before % 2) * 2 + 1), device_id_type=MESH)

    mine = pl.ds(pl.multiple_of(EDGE + core * part, 16), part)
    load_hid = [pltpu.make_async_copy(hid.at[s], rows.at[s, mine, :], hid_local.at[s]) for s in range(seqs)]
    load_small = [
        pltpu.make_async_copy(src, dst, small_local.at[n])
        for n, (src, dst) in enumerate(
            [
                (wstep, wst), (cv, ctap.at[y, 0]), (ck, ctap.at[y, 1]), (newq, qraw.at[y]),
                (jump.at[:, :, pl.ds(pl.multiple_of(y * local, 128), local)], jall.at[y]),
                (newv, nraw.at[0]), (newk, nraw.at[1]), (newg, nraw.at[2]),
            ]
        )
    ]
    load_w = [
        pltpu.make_async_copy(w.at[:, pl.ds(a * 128, 128)], w_all.at[y, a, half], w_local.at[a, half])
        for a in range(groups)
        for half, w in enumerate((wv, wk))
    ]
    for c in load_hid + load_small + load_w:
        c.start()

    sub = lax.broadcasted_iota(jnp.int32, (heads, 128), 0)
    lane = lax.broadcasted_iota(jnp.int32, (heads, 128), 1)

    def by_head(ref):
        out = jnp.zeros((heads, 128), f32)
        for h in range(heads):
            out = jnp.where(sub == h, ref[h], out)
        return out

    def by_line(value_of):
        out = jnp.zeros((lines, 128), f32)
        for a in range(groups):
            for s in range(seqs):
                pair = jnp.where(lane < 64, value_of(s, 2 * a), value_of(s, 2 * a + 1))
                out = jnp.where(sub == a * seqs + s, pair, out)
        return out

    def lines_of(x):
        x = x.astype(f32)
        return jnp.concatenate([x[:, a * 128 : (a + 1) * 128] for a in range(groups)], axis=0)

    ball[y] = jnp.where(lane == 0, by_head(bias), jnp.where(lane == 1, by_head(rate), 0.0))
    new_size = softplus(by_line(lambda s, h: newstep[s, h]) + by_line(lambda s, h: bias[h]))
    keep = jnp.exp(-by_line(lambda s, h: rate[h]) * new_size)
    pl.semaphore_wait(barrier, chips + core)

    theirs = pl.ds(pl.multiple_of(far * local, 128), local)
    send_hid = [
        send(hid.at[s], rows.at[s, mine, :], hid_send.at[s], hid_recv.at[s], core_peer) for s in range(seqs)
    ]
    send_small = [
        send(src, dst, small_send.at[n], small_recv.at[n], y_peer)
        for n, (src, dst) in enumerate(
            [
                (jump.at[:, :, theirs], jall.at[y]), (ball.at[y], ball.at[y]),
                (cv, ctap.at[y, 0]), (ck, ctap.at[y, 1]), (newq, qraw.at[y]),
            ]
        )
    ]
    edge = [
        send(
            hid.at[:, pl.ds(part - TIP, TIP), :], rows.at[:, pl.ds(EDGE - TIP, TIP), :], edge_send.at[c], edge_recv,
            (after // 2, (after % 2) * 2 + c),
        )
        for c in range(2)
    ]
    count = 2 * PIECES
    diag = groups - 1 - quarter
    first, second = (3 * count) // 8, (6 * count) // 8

    def y_copy(half, n, a, chunk, rel):
        at = pl.ds(pl.multiple_of((chunk // 2) * depth, depth), depth)
        return send(
            (wv, wk)[half].at[at, pl.ds(pl.multiple_of(a * 128, 128), 128)],
            w_all.at[y, a, half, at, :], y_send.at[n], w_recv.at[rel, chunk], y_peer,
        )

    def start_y(n):
        if isinstance(n, int):
            a, chunk, rel = (quarter, n, 0) if n < count else (diag, second + n - count, 3)
            y_copy(chunk % 2, n, a, chunk, rel).start()
        else:
            for half in range(2):

                @pl.when(n % 2 == half)
                def _():
                    y_copy(half, n, quarter, n, 0).start()

    def w_copy(a, chunk, send_sem, rel, peer):
        block = w_all.at[
            far, a, chunk % 2, pl.ds(pl.multiple_of((chunk // 2) * depth, depth), depth), :
        ]
        return send(block, block, send_sem, w_recv.at[rel, chunk], peer)

    def wait_chunk(rel, a, chunk):
        w_copy(a, chunk, y_send.at[0], rel, y_peer).wait_recv()

    def relay(chunk):
        wait_chunk(0, quarter, chunk)
        w_copy(quarter, chunk, x_send.at[chunk], 1, x_peer).start()
        w_copy(quarter, chunk, z_send.at[chunk], 2, z_peer).start()

    qx, qz = flip(quarter, 1), flip(quarter, 2)

    def relay_diag(n):
        wait_chunk(1, qx, n)
        w_copy(qx, n, z_send.at[count + n], 3, z_peer).start()
        wait_chunk(2, qz, first + n)
        w_copy(qz, first + n, x_send.at[count + n], 3, x_peer).start()

    start_y(0)
    for c in send_hid + send_small:
        c.start()

    @pl.when(core == 1)
    def _():
        for c in edge:
            c.start()

    start_y(1)
    for c in load_small:
        c.wait()
    query = lines_of(qraw[y])
    gate = lines_of(nraw[2])
    gate = gate / (1.0 + jnp.exp(-gate))
    match = jnp.sum(lines_of(nraw[1]) * query, axis=1, keepdims=True)
    coef[0] = keep * gate
    coef[1] = new_size * lines_of(nraw[0]) * match * gate

    for c in load_hid:
        c.wait()
    for c in send_hid:
        c.wait_recv()
    relay(0)
    start_y(2)
    for s in range(seqs):
        step_t[s] = (
            lax.dot_general(wst[...], rows[s, EDGE:, :], (((1,), (1,)), ((), ())), preferred_element_type=f32)
            .astype(bf16)
            .astype(f32)
        )
    for c in send_small:
        c.wait_recv()
    for b in range(2):
        for half in range(2):
            ct = ctap[b, half].astype(f32) * 0.5
            for a in range(groups):
                tall[b, a, 0 : ct.shape[0], half * 128 : (half + 1) * 128] = ct[:, a * 128 : (a + 1) * 128]
        qall[b] = lines_of(qraw[b])
    relay(1)
    start_y(3)
    decays, sizes = [], []
    for yb in range(2):
        for s in range(seqs):
            raw = step_t[s, pl.ds(pl.multiple_of((2 * yb + core) * heads, 8), heads), :]
            one = softplus(raw + ball[yb, :, 0:1])
            sizes.append(one)
            decays.append(jall[yb, s] - ball[yb, :, 1:2] * one)
    size = jnp.concatenate(sizes, axis=0)
    decay = jnp.concatenate(decays, axis=0)
    packed = jnp.zeros((heads, 128), f32)
    for n, one in enumerate(decays):
        packed = jnp.where(lane == n * heads + sub, jnp.sum(one, axis=1, keepdims=True), packed)
    totals[0] = jnp.sum(packed, axis=0, keepdims=True)
    spot = lax.broadcasted_iota(jnp.int32, decay.shape, 1)
    suffix = jnp.where(spot < local - 1, pltpu.roll(decay, local - 1, 1), 0.0)
    shift = 1
    while shift < local:
        suffix = suffix + jnp.where(spot < local - shift, pltpu.roll(suffix, local - shift, 1), 0.0)
        shift *= 2
    weight = size * jnp.exp(suffix)
    for yb in range(2):
        for s in range(seqs):
            at = (yb * seqs + s) * heads
            wrow[yb, s] = weight[at : at + heads]
    send_tot = [
        send(totals.at[0], totals.at[r], tot_send.at[r], tot_recv.at[r], chip_peer(r)) for r in range(1, chips)
    ]
    for c in send_tot:
        c.start()
    relay(2)
    start_y(4)
    edge[0].wait_recv()

    @pl.when(order == 0)
    def _():
        rows[:, 0:EDGE, :] = jnp.zeros((seqs, EDGE, width), rows.dtype)

    for c in load_w:
        c.wait()

    def project(block, a, s):
        both = jnp.dot(
            rows[s], jnp.concatenate([w_all[block, a, 0], w_all[block, a, 1]], axis=1), preferred_element_type=f32
        )
        proj[2 * s] = both[:, :128]
        proj[2 * s + 1] = both[:, 128:]

    def mixed(slab, tap):
        half = proj[slab, EDGE - 3 : EDGE - 3 + local, :] * tap[0:1]
        for k in range(1, 4):
            half = half + proj[slab, EDGE - 3 + k : EDGE - 3 + k + local, :] * tap[k : k + 1]
        return half + half * jnp.tanh(half)

    def reduce_rows(slot, block, a, s):
        tap = tall[block, a]
        key = mixed(2 * s + 1, tap[:, 128:]).astype(bf16)
        val_t = mixed(2 * s, tap[:, :128]).astype(bf16).T.astype(f32)
        spread = jnp.concatenate(
            [jnp.broadcast_to(wrow[block, s, pl.ds(2 * a + p, 1), :], (64, local)) for p in range(2)], axis=0
        )
        sfull[slot, a, s] = jnp.dot((val_t * spread).astype(bf16), key, preferred_element_type=f32)

    def group(slot, block, a):
        project(block, a, 0)
        project(block, a, 1)
        reduce_rows(slot, block, a, 0)
        reduce_rows(slot, block, a, 1)

    def flush(slot, block, a, peers):
        for s in range(seqs):
            scale = jnp.concatenate(
                [jnp.broadcast_to(fac[block, s, pl.ds(2 * a + p, 1), :], (64, 128)) for p in range(2)], axis=0
            )
            state = sfull[slot, a, s] * scale
            parts = jnp.swapaxes(state.reshape(2, sp_count, share, 128), 0, 1).reshape(sp_count, per_share, 128)
            here = pl.ds(s * per_share, per_share)
            stage[slot, a, :, here, :] = parts.astype(bf16)
            if slot == 0:
                full[a, :, here, :] = parts
            line = a * seqs + s
            q = jnp.broadcast_to(qall[block, pl.ds(line, 1), :], (16, 128)).astype(bf16)
            high = state.astype(bf16)
            low = (state - high.astype(f32)).astype(bf16)
            dims = (((1,), (1,)), ((), ()))
            read = lax.dot_general(q, high, dims, preferred_element_type=f32) + lax.dot_general(
                q, low, dims, preferred_element_type=f32
            )
            reads[slot, pl.ds(line, 1), :] = read[0:1]
        for r in peers:
            send(
                stage.at[slot, a, xor_sp(r % sp_count)], got.at[r - 1, a], st_send, st_recv, chip_peer(r)
            ).start()

    def own_block(a, carry):
        relay(3 + a)

        @pl.when(a < groups - 1)
        def _():
            start_y(5 + a)

        @pl.when(a == groups - 1)
        def _():
            start_y(count)

        @pl.when(a >= 2)
        def _():
            relay_diag(a - 2)

        group(0, y, a)
        return carry

    lax.fori_loop(0, groups, own_block, 0)
    relay(count - 1)
    start_y(count + 1)
    relay_diag(2)

    later = jnp.zeros((1, 128), f32)
    for r in range(1, chips):
        send_tot[r - 1].wait_recv()
        source = xor_sp(r % sp_count) * 2 + (far if r >= sp_count else y)
        later = later + totals[r] * jnp.where(source > order, 1.0, 0.0)
    later = jnp.broadcast_to(later, (heads, 128))
    for yb in range(2):
        for s in range(seqs):
            n = yb * seqs + s
            one = jnp.sum(jnp.where(lane == n * heads + sub, later, 0.0), axis=1, keepdims=True)
            fac[yb, s] = jnp.broadcast_to(jnp.exp(one), (heads, 128))

    def send_reads(slot, r):
        return send(reads.at[slot], read_got.at[r], rd_send.at[r], rd_recv.at[r], chip_peer(r))

    waits = {
        1: list(range(first, count)),
        2: list(range(first)) + list(range(second, count)),
        3: list(range(count)),
    }

    def far_block(k, carry):
        a = (quarter % 2 + k % 2) % 2 + 2 * ((quarter // 2 + k // 2) % 2)
        for rel, chunks in waits.items():

            @pl.when(k == rel)
            def _():
                for chunk in chunks:
                    wait_chunk(rel, a, chunk)

        @pl.when(k == groups - 1)
        def _():
            for r in range(1, sp_count):
                send_reads(0, r).start()

        group(1, far, a)
        flush(1, far, a, range(sp_count, chips))

        @pl.when(k < groups - 1)
        def _():
            flush(0, y, k, range(1, sp_count))

        @pl.when(k == groups - 2)
        def _():
            flush(0, y, groups - 1, range(1, sp_count))

        return carry

    lax.fori_loop(0, groups, far_block, 0)

    send_rd = [send_reads(r // sp_count, r) for r in range(1, chips)]
    for c in send_rd[sp_count - 1 :]:
        c.start()
    everything = send(got, got, st_send, st_recv, y_peer)
    everything.wait_recv()
    for a in range(groups):
        final = full[a, sp]
        for r in range(chips - 1):
            final = final + got[r, a].astype(f32)
        for s in range(seqs):
            for p in range(2):
                at = s * per_share + p * share
                state_out[s, 2 * a + p] = final[at : at + share].astype(bf16)
    read = reads[0]
    for r in range(1, chips):
        send_rd[r - 1].wait_recv()
        read = read + read_got[r]
    gated = coef[0] * read + coef[1]
    mean = jnp.mean(gated * gated, axis=1, keepdims=True)
    read_out[...] = gated * lax.rsqrt(mean + EPSILON)

    @pl.when(core == 1)
    def _():
        for c in edge:
            c.wait_send()

    for c in send_hid + send_small + send_tot + send_rd + [everything]:
        c.wait_send()
    for n in range(count):
        y_copy(n % 2, n, quarter, n, 0).wait_send()
        w_copy(quarter, n, x_send.at[n], 1, x_peer).wait_send()
        w_copy(quarter, n, z_send.at[n], 2, z_peer).wait_send()
    for n in range(count - second):
        y_copy((second + n) % 2, count + n, diag, second + n, 3).wait_send()
    for n in range(first):
        w_copy(qx, n, z_send.at[count + n], 3, z_peer).wait_send()
        w_copy(qz, n, x_send.at[count + n], 3, x_peer).wait_send()


def per_device(
    hidden_in, w_value, w_key, w_step, conv_value, conv_key, step_bias, decay_rate, decay_jump,
    new_value, new_key, new_query, new_gate, new_step, read_gain,
):
    sp_count, tp_count = lax.axis_size("sp"), lax.axis_size("tp")
    heads = step_bias.shape[0]
    groups = w_key.shape[1] // STATE
    seqs, part, width = hidden_in.shape
    per = heads // groups
    share = HEAD_DIM // sp_count
    if not (tp_count == 4 and groups == 4 and share == 8 and per == 2 and seqs == 2 and part % 64 == 0):
        return general(
            hidden_in, w_value, w_key, w_step, conv_value, conv_key, step_bias, decay_rate, decay_jump,
            new_value, new_key, new_query, new_gate, new_step, read_gain,
        )
    f32, bf16 = jnp.float32, jnp.bfloat16
    sp_index = lax.axis_index("sp")
    local = 2 * part
    tap_count = conv_value.shape[0]
    chips = 2 * sp_count
    block = seqs * per * share
    lines = groups * seqs
    cols = w_value.shape[1]
    vmem, anyspace = pl.BlockSpec(memory_space=pltpu.VMEM), pl.BlockSpec(memory_space=pl.ANY)
    smem = pl.BlockSpec(memory_space=pltpu.SMEM)
    dma = pltpu.SemaphoreType.DMA
    count = 2 * PIECES
    state, read = pl.pallas_call(
        mixer_kernel,
        out_shape=(
            jax.ShapeDtypeStruct((seqs, heads, share, STATE), bf16),
            jax.ShapeDtypeStruct((lines, 128), f32),
        ),
        in_specs=[anyspace] * 11 + [smem] * 3,
        out_specs=(vmem, vmem),
        scratch_shapes=[
            pltpu.VMEM((seqs, EDGE + local, width), bf16),
            pltpu.VMEM((2, groups, 2, width, 128), bf16),
            pltpu.VMEM((w_step.shape[1], width), bf16),
            pltpu.VMEM((2, 2, tap_count, cols), bf16),
            pltpu.VMEM((2, groups, 8, 256), f32),
            pltpu.VMEM((2, seqs, heads, local), f32),
            pltpu.VMEM((2, heads, 128), f32),
            pltpu.VMEM((3, seqs, cols), bf16),
            pltpu.VMEM((2, seqs, cols), bf16),
            pltpu.VMEM((2, lines, 128), f32),
            pltpu.VMEM((2, lines, 128), f32),
            pltpu.VMEM((seqs, 4 * heads, local), f32),
            pltpu.VMEM((2, seqs, heads, local), f32),
            pltpu.VMEM((4, EDGE + local, 128), f32),
            pltpu.VMEM((2, groups, seqs, 128, 128), f32),
            pltpu.VMEM((2, seqs, heads, 128), f32),
            pltpu.VMEM((chips, 1, 128), f32),
            pltpu.VMEM((2, groups, sp_count, block, 128), bf16),
            pltpu.VMEM((groups, sp_count, block, 128), f32),
            pltpu.VMEM((chips - 1, groups, block, 128), bf16),
            pltpu.VMEM((2, lines, 128), f32),
            pltpu.VMEM((chips, lines, 128), f32),
            dma((seqs,)), dma((seqs,)), dma((seqs,)), dma((groups, 2)), dma((8,)), dma((2,)), dma, dma((5,)), dma((5,)),
            dma((2 * count,)), dma((2 * count,)), dma((2 * count,)), dma((4, count)),
            dma((chips,)), dma((chips,)), dma, dma, dma((chips,)), dma((chips,)),
        ],
        compiler_params=pltpu.CompilerParams(
            collective_id=0, has_side_effects=True, vmem_limit_bytes=60 * 1024 * 1024
        ),
    )(
        hidden_in, w_value, w_key, jnp.swapaxes(w_step, 0, 1), conv_value, conv_key, jnp.swapaxes(decay_jump, 1, 2),
        new_value, new_key, new_query, new_gate, step_bias, decay_rate, new_step,
    )

    read = lax.dynamic_slice_in_dim(read.reshape(groups, seqs, per, HEAD_DIM), sp_index * share, share, 3)
    gain = lax.dynamic_slice_in_dim(read_gain.reshape(groups, 1, per, HEAD_DIM), sp_index * share, share, 3)
    read = jnp.swapaxes(read * gain.astype(f32), 0, 1)
    return state, read.reshape(seqs, heads, share).astype(bf16)


def solution(mesh):
    return jax.shard_map(
        per_device,
        mesh=mesh,
        in_specs=(
            P(None, ("sp", "tp"), None),
            P(None, "tp"),
            P(None, "tp"),
            P(),
            P(None, "tp"),
            P(None, "tp"),
            P("tp"),
            P("tp"),
            P(None, "sp", "tp"),
            P(None, "tp"),
            P(None, "tp"),
            P(None, "tp"),
            P(None, "tp"),
            P(None, "tp"),
            P("tp"),
        ),
        out_specs=(P(None, "tp", "sp", None), P(None, "tp", "sp")),
        check_vma=False,
    )
```

time: 109 us -> 67.4 us (0.62)
  Pallas kernels: 96.1 us -> 62.9 us
  other arithmetic: 7.71 us -> 0.75 us
    pallas_call x1, Pallas kernels: 96.1 us -> 62.9 us  [per_device(): pl.pallas_call(mixer_kernel, out_shape=(jax.ShapeDtypeStruct((seqs, heads...]
    another operation x3 -> x0, other arithmetic: 1.97 us -> none  [the longest x2 1.29 us: per_device(): jnp.stack([per_channel(jnp.exp(-decay_rate * new_size)) * gate, per_chann...]
    mul x2 -> x1, other arithmetic: 1.53 us -> 0.08 us  [per_device(): read = jnp.swapaxes(read * gain.astype(f32), 0, 1)]
where the time goes in v2:
time: 67.4 us; the launch traced here: 67.2 us
  Pallas kernels  62.9 us (93%)
  local copies, waits for them, and re-layouts  2.89 us (4%)
  other arithmetic  0.75 us (1%)
    pallas_call x1, Pallas kernels, per_device(): pl.pallas_call(mixer_kernel, out_shape=(jax.ShapeDtypeStruct((seqs, heads...  62.9 us
    unnamed x1, local copies, waits for them, and re-layouts  1.37 us

profile of v2, /device:TPU:0, one launch (start us, length us, event | category | flops | bytes accessed | tf_op | source)
XLA Modules:
  0.0 67.2 jit_solution(6523548582778884721)
XLA Ops:
  0.6 0.8 %reshape.13 = bf16[4,1,2,64]{3,2,0,1:T(2,128)(2,1)S(1)} reshape(bf16[512]{0:T(512)(128)(2,1)} %param.29) | data formatting | bytes 2048 | tf_op jit(solution)/shard_map/reshape | solution.py:633
  1.4 0.1 bitcast_convert_fusion
  1.5 62.9 %shard_map.158 = (bf16[2,8,8,128]{3,2,1,0:T(8,128)(2,1)}, f32[8,128]{1,0:T(8,128)}) custom-call(bf16[2,384,2048]{2,1,0:T(8,128)(2,1)} %hid.1, bf16[2048,512]{1,0:T(8,128)(2,1)} %wv.1, bf16[2048,512]{1,0:T(8,128)(2,1)} %wk.1, bf16[32,2048]{1,0:T(8,128)(2,1)} %bitcast.8, bf16[4,512]{1,0:T(4,128)(2,1)} %cv.1, bf16[4,512]{1,0:T(4,128)(2,1)} %ck.1, ...), custom_call_target="tpu_custom_call" | custom-call | tf_op jit(solution)/shard_map/pallas_call | solution.py:589
  64.3 0.8 %reshape.12 = f32[4,2,2,64]{3,2,1,0:T(2,128)S(1)} reshape(f32[8,128]{1,0:T(8,128)} %get-tuple-element.5) | data formatting | bytes 8192 | tf_op jit(solution)/shard_map/reshape | solution.py:632
  65.1 0.7 %fusion = bf16[4,2,2,8]{3,2,0,1:T(2,128)(2,1)} fusion(f32[4,2,8]{2,1,0:T(2,128)S(1)} %bitcast_convert_fusion, f32[4,2,2,64]{3,2,1,0:T(2,128)S(1)} %reshape.12, s32[]{:T(128)S(6)} %select_n.4), kind=kLoop, calls=%fused_computation.1 | loop fusion | flops 256 | bytes 4612 | tf_op jit(solution)/shard_map/convert_element_type | solution.py:635
  65.8 1.4 %copy.23 = bf16[2,8,8,128]{3,2,1,0:T(8,128)(2,1)} copy(bf16[2,8,8,128]{3,2,1,0:T(8,128)(2,1)} %get-tuple-element.8) | data formatting | bytes 65536

commit v3 on v2

--- a/solution.py
+++ b/solution.py
@@ -134,7 +134,8 @@
 
 
 MESH = pl.DeviceIdType.MESH
-PIECES = 4
+PIECES = 8
+Y_AHEAD = 4
 EDGE = 16
 TIP = 8
 
@@ -148,9 +149,9 @@
 
 
 def mixer_kernel(
-    hid, wv, wk, wstep, cv, ck, jump, newv, newk, newq, newg, bias, rate, newstep,
+    hid, wv, wk, wstep, cv, ck, jump, newv, newk, newq, newg, gain, bias, rate, newstep,
     state_out, read_out,
-    rows, w_all, wst, ctap, tall, jall, ball, nraw, qraw, qall, coef, step_t, wrow, proj, sfull, fac, totals,
+    rows, w_all, wst, gvec, ctap, tall, jall, ball, nraw, qraw, qall, coef, step_t, wrow, proj, sfull, fac, totals,
     stage, full, got, reads, read_got,
     hid_local, hid_send, hid_recv, w_local, small_local, edge_send, edge_recv, small_send, small_recv,
     y_send, x_send, z_send, w_recv, tot_send, tot_recv, st_send, st_recv, rd_send, rd_recv,
@@ -211,7 +212,7 @@
             [
                 (wstep, wst), (cv, ctap.at[y, 0]), (ck, ctap.at[y, 1]), (newq, qraw.at[y]),
                 (jump.at[:, :, pl.ds(pl.multiple_of(y * local, 128), local)], jall.at[y]),
-                (newv, nraw.at[0]), (newk, nraw.at[1]), (newg, nraw.at[2]),
+                (newv, nraw.at[0]), (newk, nraw.at[1]), (newg, nraw.at[2]), (gain, gvec),
             ]
         )
     ]
@@ -271,7 +272,8 @@
     ]
     count = 2 * PIECES
     diag = groups - 1 - quarter
-    first, second = (3 * count) // 8, (6 * count) // 8
+    z_part, second = count // 4, count // 4 + (5 * count) // 16
+    x_part, y_part = second - z_part, count - second
 
     def y_copy(half, n, a, chunk, rel):
         at = pl.ds(pl.multiple_of((chunk // 2) * depth, depth), depth)
@@ -281,15 +283,15 @@
         )
 
     def start_y(n):
-        if isinstance(n, int):
-            a, chunk, rel = (quarter, n, 0) if n < count else (diag, second + n - count, 3)
-            y_copy(chunk % 2, n, a, chunk, rel).start()
-        else:
-            for half in range(2):
-
-                @pl.when(n % 2 == half)
-                def _():
-                    y_copy(half, n, quarter, n, 0).start()
+        for half in range(2):
+
+            @pl.when(jnp.logical_and(n < count, n % 2 == half))
+            def _():
+                y_copy(half, n, quarter, n, 0).start()
+
+            @pl.when(jnp.logical_and(n >= count, (n - count + second) % 2 == half))
+            def _():
+                y_copy(half, n, diag, n - count + second, 3).start()
 
     def w_copy(a, chunk, send_sem, rel, peer):
         block = w_all.at[
@@ -305,15 +307,22 @@
         w_copy(quarter, chunk, x_send.at[chunk], 1, x_peer).start()
         w_copy(quarter, chunk, z_send.at[chunk], 2, z_peer).start()
 
+        @pl.when(chunk + Y_AHEAD < count + y_part)
+        def _():
+            start_y(chunk + Y_AHEAD)
+
     qx, qz = flip(quarter, 1), flip(quarter, 2)
 
     def relay_diag(n):
-        wait_chunk(1, qx, n)
-        w_copy(qx, n, z_send.at[count + n], 3, z_peer).start()
-        wait_chunk(2, qz, first + n)
-        w_copy(qz, first + n, x_send.at[count + n], 3, x_peer).start()
+        if n < z_part:
+            wait_chunk(1, qx, n)
+            w_copy(qx, n, z_send.at[count + n], 3, z_peer).start()
+        if n < x_part:
+            wait_chunk(2, qz, z_part + n)
+            w_copy(qz, z_part + n, x_send.at[count + n], 3, x_peer).start()
 
     start_y(0)
+    start_y(1)
     for c in send_hid + send_small:
         c.start()
 
@@ -322,7 +331,8 @@
         for c in edge:
             c.start()
 
-    start_y(1)
+    for n in range(2, Y_AHEAD):
+        start_y(n)
     for c in load_small:
         c.wait()
     query = lines_of(qraw[y])
@@ -331,13 +341,18 @@
     match = jnp.sum(lines_of(nraw[1]) * query, axis=1, keepdims=True)
     coef[0] = keep * gate
     coef[1] = new_size * lines_of(nraw[0]) * match * gate
-
+    gains = jnp.zeros((lines, 128), f32)
+    for a in range(groups):
+        one = gvec[a * 128 : (a + 1) * 128].astype(f32).reshape(1, 128)
+        gains = jnp.where(sub // seqs == a, jnp.broadcast_to(one, (lines, 128)), gains)
+    coef[2] = gains
+
+    relay(0)
     for c in load_hid:
         c.wait()
     for c in send_hid:
         c.wait_recv()
-    relay(0)
-    start_y(2)
+    relay(1)
     for s in range(seqs):
         step_t[s] = (
             lax.dot_general(wst[...], rows[s, EDGE:, :], (((1,), (1,)), ((), ())), preferred_element_type=f32)
@@ -352,8 +367,7 @@
             for a in range(groups):
                 tall[b, a, 0 : ct.shape[0], half * 128 : (half + 1) * 128] = ct[:, a * 128 : (a + 1) * 128]
         qall[b] = lines_of(qraw[b])
-    relay(1)
-    start_y(3)
+    relay(2)
     decays, sizes = [], []
     for yb in range(2):
         for s in range(seqs):
@@ -383,8 +397,7 @@
     ]
     for c in send_tot:
         c.start()
-    relay(2)
-    start_y(4)
+    relay(3)
     edge[0].wait_recv()
 
     @pl.when(order == 0)
@@ -448,27 +461,18 @@
             ).start()
 
     def own_block(a, carry):
-        relay(3 + a)
-
-        @pl.when(a < groups - 1)
-        def _():
-            start_y(5 + a)
-
-        @pl.when(a == groups - 1)
-        def _():
-            start_y(count)
-
-        @pl.when(a >= 2)
-        def _():
-            relay_diag(a - 2)
-
+        relay(4 + 2 * a)
+        relay(5 + 2 * a)
         group(0, y, a)
         return carry
 
     lax.fori_loop(0, groups, own_block, 0)
-    relay(count - 1)
-    start_y(count + 1)
-    relay_diag(2)
+    for n in range(4 + 2 * groups, count):
+        relay(n)
+    for n in range(count + Y_AHEAD, count + y_part):
+        start_y(n)
+    for n in range(max(z_part, x_part)):
+        relay_diag(n)
 
     later = jnp.zeros((1, 128), f32)
     for r in range(1, chips):
@@ -486,8 +490,8 @@
         return send(reads.at[slot], read_got.at[r], rd_send.at[r], rd_recv.at[r], chip_peer(r))
 
     waits = {
-        1: list(range(first, count)),
-        2: list(range(first)) + list(range(second, count)),
+        1: list(range(z_part, count)),
+        2: list(range(z_part)) + list(range(second, count)),
         3: list(range(count)),
     }
 
@@ -539,7 +543,12 @@
         read = read + read_got[r]
     gated = coef[0] * read + coef[1]
     mean = jnp.mean(gated * gated, axis=1, keepdims=True)
-    read_out[...] = gated * lax.rsqrt(mean + EPSILON)
+    normed = gated * lax.rsqrt(mean + EPSILON) * coef[2]
+    left = pltpu.roll(normed, 128 - sp * share, 1)
+    right = pltpu.roll(left, 64, 1)
+    even = sub % 2 == 0
+    read_out[0] = jnp.where(even, left, pltpu.roll(right, 1, 0))[:, :share].astype(bf16)
+    read_out[1] = jnp.where(even, pltpu.roll(left, lines - 1, 0), right)[:, :share].astype(bf16)
 
     @pl.when(core == 1)
     def _():
@@ -552,11 +561,12 @@
         y_copy(n % 2, n, quarter, n, 0).wait_send()
         w_copy(quarter, n, x_send.at[n], 1, x_peer).wait_send()
         w_copy(quarter, n, z_send.at[n], 2, z_peer).wait_send()
-    for n in range(count - second):
+    for n in range(y_part):
         y_copy((second + n) % 2, count + n, diag, second + n, 3).wait_send()
-    for n in range(first):
+    for n in range(z_part):
         w_copy(qx, n, z_send.at[count + n], 3, z_peer).wait_send()
-        w_copy(qz, n, x_send.at[count + n], 3, x_peer).wait_send()
+    for n in range(x_part):
+        w_copy(qz, z_part + n, x_send.at[count + n], 3, x_peer).wait_send()
 
 
 def per_device(
@@ -575,7 +585,6 @@
             new_value, new_key, new_query, new_gate, new_step, read_gain,
         )
     f32, bf16 = jnp.float32, jnp.bfloat16
-    sp_index = lax.axis_index("sp")
     local = 2 * part
     tap_count = conv_value.shape[0]
     chips = 2 * sp_count
@@ -590,14 +599,15 @@
         mixer_kernel,
         out_shape=(
             jax.ShapeDtypeStruct((seqs, heads, share, STATE), bf16),
-            jax.ShapeDtypeStruct((lines, 128), f32),
+            jax.ShapeDtypeStruct((seqs, heads, share), bf16),
         ),
-        in_specs=[anyspace] * 11 + [smem] * 3,
+        in_specs=[anyspace] * 12 + [smem] * 3,
         out_specs=(vmem, vmem),
         scratch_shapes=[
             pltpu.VMEM((seqs, EDGE + local, width), bf16),
             pltpu.VMEM((2, groups, 2, width, 128), bf16),
             pltpu.VMEM((w_step.shape[1], width), bf16),
+            pltpu.VMEM((cols,), bf16),
             pltpu.VMEM((2, 2, tap_count, cols), bf16),
             pltpu.VMEM((2, groups, 8, 256), f32),
             pltpu.VMEM((2, seqs, heads, local), f32),
@@ -605,7 +615,7 @@
             pltpu.VMEM((3, seqs, cols), bf16),
             pltpu.VMEM((2, seqs, cols), bf16),
             pltpu.VMEM((2, lines, 128), f32),
-            pltpu.VMEM((2, lines, 128), f32),
+            pltpu.VMEM((3, lines, 128), f32),
             pltpu.VMEM((seqs, 4 * heads, local), f32),
             pltpu.VMEM((2, seqs, heads, local), f32),
             pltpu.VMEM((4, EDGE + local, 128), f32),
@@ -617,7 +627,7 @@
             pltpu.VMEM((chips - 1, groups, block, 128), bf16),
             pltpu.VMEM((2, lines, 128), f32),
             pltpu.VMEM((chips, lines, 128), f32),
-            dma((seqs,)), dma((seqs,)), dma((seqs,)), dma((groups, 2)), dma((8,)), dma((2,)), dma, dma((5,)), dma((5,)),
+            dma((seqs,)), dma((seqs,)), dma((seqs,)), dma((groups, 2)), dma((9,)), dma((2,)), dma, dma((5,)), dma((5,)),
             dma((2 * count,)), dma((2 * count,)), dma((2 * count,)), dma((4, count)),
             dma((chips,)), dma((chips,)), dma, dma, dma((chips,)), dma((chips,)),
         ],
@@ -626,13 +636,10 @@
         ),
     )(
         hidden_in, w_value, w_key, jnp.swapaxes(w_step, 0, 1), conv_value, conv_key, jnp.swapaxes(decay_jump, 1, 2),
-        new_value, new_key, new_query, new_gate, step_bias, decay_rate, new_step,
-    )
-
-    read = lax.dynamic_slice_in_dim(read.reshape(groups, seqs, per, HEAD_DIM), sp_index * share, share, 3)
-    gain = lax.dynamic_slice_in_dim(read_gain.reshape(groups, 1, per, HEAD_DIM), sp_index * share, share, 3)
-    read = jnp.swapaxes(read * gain.astype(f32), 0, 1)
-    return state, read.reshape(seqs, heads, share).astype(bf16)
+        new_value, new_key, new_query, new_gate, read_gain, step_bias, decay_rate, new_step,
+    )
+
+    return state, read
 
 
 def solution(mesh):

time: 67.4 us -> 62.7 us (0.930)
  Pallas kernels: 62.9 us -> 59.1 us
  other arithmetic: 0.75 us -> 0 us
    pallas_call x1, Pallas kernels: 62.9 us -> 59.1 us  [per_device(): pl.pallas_call(mixer_kernel, out_shape=(jax.ShapeDtypeStruct((seqs, heads...]
    reshape x2 -> x0, local copies, waits for them, and re-layouts: 1.52 us -> none  [the longest x1 0.76 us: per_device(): read_gain.reshape(groups, 1, per, HEAD_DIM)]
    unnamed x1 -> x2, local copies, waits for them, and re-layouts: 1.37 us -> 2.65 us
where the time goes in v3:
time: 62.7 us; the launch traced here: 62.4 us
  Pallas kernels  59.1 us (94%)
  local copies, waits for them, and re-layouts  2.65 us (4%)
  between operations  0.64 us (1%)
    pallas_call x1, Pallas kernels, per_device(): pl.pallas_call(mixer_kernel, out_shape=(jax.ShapeDtypeStruct((seqs, heads...  59.1 us
    unnamed x2, local copies, waits for them, and re-layouts  2.65 us

profile of v3, /device:TPU:0, one launch (start us, length us, event | category | flops | bytes accessed | tf_op | source)
XLA Modules:
  0.0 62.4 jit_solution(16859331123022679155)
XLA Ops:
  0.6 59.1 %shard_map.158 = (bf16[2,8,8,128]{3,2,1,0:T(8,128)(2,1)}, bf16[2,8,8]{2,1,0:T(8,128)(2,1)}) custom-call(bf16[2,384,2048]{2,1,0:T(8,128)(2,1)} %hid.1, bf16[2048,512]{1,0:T(8,128)(2,1)} %wv.1, bf16[2048,512]{1,0:T(8,128)(2,1)} %wk.1, bf16[32,2048]{1,0:T(8,128)(2,1)} %bitcast.2, bf16[4,512]{1,0:T(4,128)(2,1)} %cv.1, bf16[4,512]{1,0:T(4,128)(2,1)} %ck.1, ...), custom_call_target="tpu_custom_call" | custom-call | tf_op jit(solution)/shard_map/pallas_call | solution.py:598
  59.8 1.4 %copy.19 = bf16[2,8,8,128]{3,2,1,0:T(8,128)(2,1)} copy(bf16[2,8,8,128]{3,2,1,0:T(8,128)(2,1)} %get-tuple-element.4) | data formatting | bytes 65536
  61.2 1.3 %copy.20 = bf16[2,8,8]{2,1,0:T(8,128)(2,1)} copy(bf16[2,8,8]{2,1,0:T(8,128)(2,1)} %get-tuple-element.5) | data formatting | bytes 512
